TPU v7x, 128 devices: a whole 4x4x4 slice. The times are simulated.
128 devices in a mesh: sp: 16 (over z, x), tp: 8 (over y, core).
Axes of the slice: x: 4, y: 4, z: 4, core: 2. Of those that a mesh axis runs over, the one named last changes fastest.
Arguments:
- queries: bfloat16 [16384, 1024], P('sp', 'tp'), may hold values from -75 to 75
- key_rows: bfloat16 [16384, 1024], P('sp', 'tp'), may hold values from -4 to 4
- value_rows: bfloat16 [16384, 1024], P('sp', 'tp'), may hold values from -6 to 6
- cum_gate: float32 [16, 16384], P('tp'), may hold values from -2342 to 0, as said below
- residual: bfloat16 [16384, 2048], P(('sp', 'tp')), may hold values from -6 to 6
- out_weight: bfloat16 [1024, 2048], replicated, may hold values from -0.1875 to 0.1875
- gain_mix: float32 [2048], replicated, may hold values from 0.1 to 1.9
- gain_pre: float32 [2048], replicated, may hold values from 0.1 to 1.9
- gain_post: float32 [2048], replicated, may hold values from 0.1 to 1.9
- route_ids: int32 [16384, 2], P(('sp', 'tp')), may hold values from 0 to 127, all different within a row; in each aligned block of 128 rows (0 to 127, 128 to 255, ...) at most 3 rows name the same one
- route_weight: float32 [16384, 2], P(('sp', 'tp')), may hold values from 0.2 to 1
- w_gate: bfloat16 [128, 2048, 512], P(('sp', 'tp')), may hold values from -0.125 to 0.125
- w_up: bfloat16 [128, 2048, 512], P(('sp', 'tp')), may hold values from -0.125 to 0.125
- w_down: bfloat16 [128, 512, 2048], P(('sp', 'tp')), may hold values from -0.25 to 0.25
Outputs:
- layer_out: bfloat16 [16384, 2048], P(('sp', 'tp'))
Inputs may be any that keep to these rules, and one draw needn't show every extreme that they name: `route_ids`: each row names 2 different experts; in the rows of one device no expert is named more than 3 times, a bound that some block reaches. `cum_gate`: along the positions each head's values never rise.
All inputs are finite; a program needn't handle non-finite values.
Results may differ from a plain program's by a relative error of at most 0.018.
Values may be sent and summed in bfloat16 or wider, within the bound.
A program may use at most 64 MiB of HBM per device.

v0:
```python
import math
import jax
import jax.numpy as jnp
from jax import lax
from jax.sharding import PartitionSpec as P

HEAD_DIM = 64
NORM_EPS = 1e-06
MASKED = -1e30


def rms_scale(rows, gain):
    mean_sq = jnp.mean(rows * rows, axis=-1, keepdims=True)
    return rows * lax.rsqrt(mean_sq + NORM_EPS) * gain


def attend(running, queries, gate_q, q_start, key_part, value_part, gate_k, k_start):
    row_peak, row_total, weighted = running
    scores = jnp.einsum(
        "qhd,khd->hqk", queries, key_part, preferred_element_type=jnp.float32
    ) * HEAD_DIM ** (-0.5)
    scores = scores + gate_q[:, :, None] - gate_k[:, None, :]
    query_pos = q_start + lax.iota(jnp.int32, queries.shape[0])
    key_pos = k_start + lax.iota(jnp.int32, key_part.shape[0])
    allowed = (key_pos[None, :] <= query_pos[:, None])[None]
    scores = jnp.where(allowed, scores, MASKED)
    new_peak = jnp.maximum(row_peak, jnp.max(scores, axis=-1))
    unnorm = jnp.where(allowed, jnp.exp(scores - new_peak[..., None]), 0.0)
    rescale = jnp.exp(row_peak - new_peak)
    row_total = row_total * rescale + jnp.sum(unnorm, axis=-1)
    weighted = weighted * rescale.T[:, :, None] + jnp.einsum(
        "hqk,khd->qhd", unnorm.astype(jnp.bfloat16), value_part, preferred_element_type=jnp.float32
    )
    return (new_peak, row_total, weighted)


def local(
    queries,
    key_rows,
    value_rows,
    cum_gate,
    residual,
    out_weight,
    gain_mix,
    gain_pre,
    gain_post,
    route_ids,
    route_weight,
    w_gate,
    w_up,
    w_down,
):
    tok_dev, feature_width = queries.shape
    local_heads = feature_width // HEAD_DIM
    my_start = lax.axis_index("sp") * tok_dev
    query_heads = queries.reshape(tok_dev, local_heads, HEAD_DIM)
    gate_q = lax.dynamic_slice_in_dim(cum_gate, my_start, tok_dev, 1)
    initial = (
        jnp.full((local_heads, tok_dev), MASKED, jnp.float32),
        jnp.zeros((local_heads, tok_dev), jnp.float32),
        jnp.zeros((tok_dev, local_heads, HEAD_DIM), jnp.float32),
    )
    paired = jnp.stack((key_rows, value_rows))

    def consume(running, key_part, value_part, k_start):
        row_count = key_part.shape[0]
        gate_k = lax.dynamic_slice_in_dim(cum_gate, k_start, row_count, 1)
        return attend(
            running,
            query_heads,
            gate_q,
            my_start,
            key_part.reshape(row_count, local_heads, HEAD_DIM),
            value_part.reshape(row_count, local_heads, HEAD_DIM),
            gate_k,
            k_start,
        )

    running = initial
    piece = lax.all_gather(paired, "sp", axis=1, tiled=True)
    row_count = piece.shape[1]
    span_rows = math.gcd(row_count, tok_dev)

    def single(block_index, running):
        offset = block_index * span_rows
        part = lax.dynamic_slice_in_dim(piece, offset, span_rows, 1)
        return lax.cond(
            offset < my_start + tok_dev,
            lambda state_now: consume(state_now, part[0], part[1], offset),
            lambda state_now: state_now,
            running,
        )

    running = lax.fori_loop(0, row_count // span_rows, single, running)
    row_peak, row_total, weighted = running
    attended = (
        (weighted / row_total.T[:, :, None]).astype(jnp.bfloat16).reshape(tok_dev, feature_width)
    )
    head_rows = lax.all_to_all(attended, "tp", split_axis=0, concat_axis=1, tiled=True)
    projected = jnp.dot(head_rows, out_weight, preferred_element_type=jnp.float32)
    stream = (residual.astype(jnp.float32) + rms_scale(projected, gain_mix)).astype(jnp.bfloat16)
    stream_wide = lax.optimization_barrier(stream).astype(jnp.float32)
    normed = rms_scale(stream_wide, gain_pre).astype(jnp.bfloat16)
    rows_dev, top_count = route_ids.shape
    model_width = normed.shape[1]
    experts_all = lax.axis_size("sp") * lax.axis_size("tp")
    capacity = max(2, (4 * rows_dev * top_count + 3 * experts_all - 1) // (3 * experts_all))
    flat_ids = route_ids.reshape(-1)
    onehot = (flat_ids[:, None] == lax.iota(jnp.int32, experts_all)[None, :]).astype(jnp.int32)
    slot_rank = jnp.sum(jnp.cumsum(onehot, axis=0) * onehot, axis=1) - 1
    slot_index = flat_ids * capacity + slot_rank
    spread = jnp.repeat(normed, top_count, axis=0)
    outgoing = (
        jnp.zeros((experts_all * capacity, model_width), jnp.bfloat16).at[slot_index].set(spread)
    )
    outgoing = outgoing.reshape(experts_all, capacity, model_width)
    arrived = lax.all_to_all(outgoing, ("sp", "tp"), split_axis=0, concat_axis=0, tiled=True)
    sources, slots, width_here = arrived.shape
    flat_rows = arrived.reshape(sources * slots, width_here)
    gate_act = jnp.dot(flat_rows, w_gate[0], preferred_element_type=jnp.float32)
    up_act = jnp.dot(flat_rows, w_up[0], preferred_element_type=jnp.float32)
    hidden = (jax.nn.silu(gate_act) * up_act).astype(jnp.bfloat16)
    expert_out = jnp.dot(hidden, w_down[0], preferred_element_type=jnp.float32).astype(jnp.bfloat16)
    returned = lax.all_to_all(
        expert_out.reshape(sources, slots, width_here),
        ("sp", "tp"),
        split_axis=0,
        concat_axis=0,
        tiled=True,
    )
    picked = returned.reshape(experts_all * capacity, model_width)[slot_index]
    picked = picked.reshape(rows_dev, top_count, model_width).astype(jnp.float32)
    combined = jnp.sum(picked * route_weight[:, :, None], axis=1)
    return (stream_wide + rms_scale(combined, gain_post)).astype(jnp.bfloat16)


def solution(mesh):
    return jax.shard_map(
        local,
        mesh=mesh,
        in_specs=(
            P("sp", "tp"),
            P("sp", "tp"),
            P("sp", "tp"),
            P("tp", None),
            P(("sp", "tp"), None),
            P(),
            P(),
            P(),
            P(),
            P(("sp", "tp"), None),
            P(("sp", "tp"), None),
            P(("sp", "tp"), None, None),
            P(("sp", "tp"), None, None),
            P(("sp", "tp"), None, None),
        ),
        out_specs=P(("sp", "tp"), None),
        check_vma=False,
    )
```

profile of v0, /device:TPU:1, one launch (start us, length us, event | category | flops | bytes accessed | tf_op | source)
XLA Modules:
  0.0 409.1 jit_solution(8245087762462546506)
XLA Ops:
  13.2 70.6 %all-gather.2.cloned.1.call-done = bf16[2,16384,128]{1,2,0:T(8,128)(2,1)} async-done(((bf16[2,1024,128]{1,2,0:T(8,128)(2,1)}), bf16[2,16384,128]{1,2,0:T(8,128)(2,1)}) %all-gather.2.cloned.1.call-update) | async-done | bytes 8388624 | tf_op jit(solution)/shard_map/all_gather | solution.py:80
  84.0 11.8 %while.18 = (s32[]{:T(128)}, f32[2,1024]{1,0:T(2,128)S(1)}, f32[2,1024]{1,0:T(2,128)S(1)}, f32[1024,2,64]{0,2,1:T(8,128)S(1)}, s32[]{:T(128)}, /*index=5*/s32[]{...) while((s32[]{:T(128)}, f32[2,1024]{1,0:T(2,128)S(1)}, ...), condition=%wide.region_5.6_spmd, body=%wide.region_0.5_spmd.sunk | while | flops 578035712 | bytes 32457040 | solution.py:94
  84.0 11.1 %conditional.2 = ((f32[2,1024]{1,0:T(2,128)S(1)}, f32[2,1024]{1,0:T(2,128)S(1)}, f32[1024,2,64]{0,2,1:T(8,128)S(1)})) conditional(s32[]{:T(128)} %convert_element_type.89, (f32[2,1024]{1,0:T(2,128)S(1)}, f32[2,1024]{1,0:T(2,128)S(1)}, f32[1024,2,64]{0,2,1:T(8,128)S(1)}) %tuple.52, (s32[]{:T(128)}, s32[]{:T(128)}, bf16[2,16384,128]{1,2,0:T(8,128)(2,1)}, ...), branch_computations={%region_1.0_spmd, %region_2.4_spmd} | conditional | flops 578035712 | bytes 32456802 | solution.py:87
  86.4 2.4 fusion.2
  88.9 3.2 fusion.9
  92.1 3.0 fusion.1
  96.6 5.1 %all-to-all-start = ((bf16[8,128,128]{1,2,0:T(8,128)(2,1)}), bf16[8,128,128]{1,2,0:T(8,128)(2,1)S(1)}, u32[]{:S(2)}, u32[]{:S(2)}) async-start(bf16[8,128,128]{1,2,0:T(8,128)(2,1)} %copy.45), calls=%async_computation | async-start | bytes 524288 | tf_op jit(solution)/shard_map/all_to_all | solution.py:99
  102.0 6.2 %all-to-all-done = bf16[8,128,128]{1,2,0:T(8,128)(2,1)S(1)} async-done(((bf16[8,128,128]{1,2,0:T(8,128)(2,1)}), bf16[8,128,128]{1,2,0:T(8,128)(2,1)S(1)}, u32[]{:S(2)}, u32[]{:S(2)}) %all-to-all-start) | async-done | bytes 262176 | tf_op jit(solution)/shard_map/all_to_all | solution.py:99
  108.2 3.0 multiply_reduce_fusion.2
  111.9 1.7 broadcast_in_dim.62
  113.6 2.3 reshape.167
  115.8 4.1 %scatter_custom_fusion = bf16[384,2048]{1,0:T(8,128)(2,1)} fusion(s32[256]{0:T(256)S(1)} %bitcast.80, bf16[256,2048]{1,0:T(8,128)(2,1)} %reshape.167, bf16[]{:T(256)} %constant.98.clone.1), kind=kCustom, calls=%fused_computation.47 | custom fusion | bytes 1573376 | tf_op jit(solution)/shard_map/scatter | solution.py:114
  120.0 5.1 %reshape.150 = bf16[128,3,2048]{2,1,0:T(4,128)(2,1)} reshape(bf16[384,2048]{1,0:T(8,128)(2,1)} %scatter_custom_fusion) | data formatting | bytes 3145728 | tf_op jit(solution)/shard_map/reshape | solution.py:116
  125.1 202.5 %all_to_all.29 = bf16[128,3,2048]{2,1,0:T(4,128)(2,1)} all-to-all(bf16[128,3,2048]{2,1,0:T(4,128)(2,1)} %reshape.150), channel_id=1, replica_groups=mesh['sp'=16,'tp'=8] {'sp','tp'}, dimensions={0} | all-to-all | bytes 3145728 | tf_op jit(solution)/shard_map/all_to_all | solution.py:117
  327.6 5.0 %reshape.151 = bf16[384,2048]{1,0:T(8,128)(2,1)} reshape(bf16[128,3,2048]{2,1,0:T(4,128)(2,1)} %all_to_all.29) | data formatting | bytes 3145728 | tf_op jit(solution)/shard_map/reshape | solution.py:119
  332.7 3.9 fusion.19
  336.6 5.3 %convolution_convert_fusion = bf16[384,2048]{1,0:T(8,128)(2,1)} fusion(bf16[1,512,2048]{2,1,0:T(8,128)(2,1)S(1)} %copy-done, bf16[384,2048]{1,0:T(8,128)(2,1)} %reshape.151, bf16[1,2048,512]{2,1,0:T(8,128)(2,1)} %param.30, f32[384,512]{1,0:T(8,128)} %fusion.19), kind=kOutput, calls=%fused_computation.23 | convolution fusion | flops 1612578816 | bytes 8126464 | tf_op jit(solution)/shard_map/dot_general | solution.py:123
  341.9 5.2 %reshape.152 = bf16[128,3,2048]{2,1,0:T(4,128)(2,1)} reshape(bf16[384,2048]{1,0:T(8,128)(2,1)} %convolution_convert_fusion) | data formatting | bytes 3145728 | tf_op jit(solution)/shard_map/reshape | solution.py:125
  347.1 5.8 %all-to-all-start.2 = ((bf16[128,3,2048]{2,1,0:T(4,128)(2,1)}), bf16[128,3,2048]{2,1,0:T(4,128)(2,1)}, u32[]{:S(2)}, u32[]{:S(2)}) async-start(bf16[128,3,2048]{2,1,0:T(4,128)(2,1)} %reshape.152), calls=%async_computation.2 | async-start | bytes 4194304 | tf_op jit(solution)/shard_map/all_to_all | solution.py:124
  353.0 29.7 %all-to-all-done.2 = bf16[128,3,2048]{2,1,0:T(4,128)(2,1)} async-done(((bf16[128,3,2048]{2,1,0:T(4,128)(2,1)}), bf16[128,3,2048]{2,1,0:T(4,128)(2,1)}, u32[]{:S(2)}, u32[]{:S(2)}) %all-to-all-start.2) | async-done | bytes 1572896 | tf_op jit(solution)/shard_map/all_to_all | solution.py:124
  382.8 5.1 %reshape.153 = bf16[384,2048]{1,0:T(8,128)(2,1)} reshape(bf16[128,3,2048]{2,1,0:T(4,128)(2,1)} %all-to-all-done.2) | data formatting | bytes 3145728 | tf_op jit(solution)/shard_map/reshape | solution.py:131
  387.9 4.9 %gather_fusion = bf16[256,2048]{1,0:T(8,128)(2,1)} fusion(bf16[384,2048]{1,0:T(8,128)(2,1)} %reshape.153, s32[1024]{0:T(1024)S(1)} %pad_clamp_fusion), kind=kCustom, calls=%fused_computation | custom fusion | bytes 2098176 | tf_op jit(solution)/shard_map/gather | solution.py:131
  392.8 3.4 reshape.154
  396.2 4.8 %multiply_reduce_fusion = f32[128,2048]{1,0:T(8,128)S(1)} fusion(f32[128,2,2048]{2,1,0:T(2,128)} %reshape.154, f32[128,2]{1,0:T(8,128)S(1)} %copy.51), kind=kLoop, calls=%fused_computation.29 | loop fusion | flops 786432 | bytes 3146752 | tf_op jit(solution)/shard_map/reduce_sum | solution.py:133
  (76 shorter events, 12.4 us)
Async XLA Ops:
  6.5 330.1 %copy-start = (bf16[1,512,2048]{2,1,0:T(8,128)(2,1)S(1)}, bf16[1,512,2048]{2,1,0:T(8,128)(2,1)}, u32[]{:S(2)}) copy-start(bf16[1,512,2048]{2,1,0:T(8,128)(2,1)} %param.31) | copy-start | bytes 6291460
  6.5 6.7 %copy-start.5 = (s32[128,2]{0,1:T(2,128)S(1)}, s32[128,2]{0,1:T(2,128)}, u32[]{:S(2)}) copy-start(s32[128,2]{0,1:T(2,128)} %param.27) | copy-start | bytes 3076
  6.5 77.3 %all-gather.2.cloned.1.call-start = ((), (), s32[]{:S(2)}) async-start(), calls=%async_computation.3 | async-start | bytes 8912896 | tf_op jit(solution)/shard_map/all_gather | solution.py:80
  95.8 15.5 %copy-start.1 = (bf16[128,2048]{1,0:T(8,128)(2,1)S(1)}, bf16[128,2048]{1,0:T(8,128)(2,1)}, u32[]{:S(2)}) copy-start(bf16[128,2048]{1,0:T(8,128)(2,1)} %param.22) | copy-start | bytes 1572868
  95.8 15.5 %copy-start.2 = (f32[2048]{0:T(1024)S(1)}, f32[2048]{0:T(1024)}, u32[]{:S(2)}) copy-start(f32[2048]{0:T(1024)} %param.24) | copy-start | bytes 24580
  96.6 11.6 %all-to-all-start = ((bf16[8,128,128]{1,2,0:T(8,128)(2,1)}), bf16[8,128,128]{1,2,0:T(8,128)(2,1)S(1)}, u32[]{:S(2)}, u32[]{:S(2)}) async-start(bf16[8,128,128]{1,2,0:T(8,128)(2,1)} %copy.45), calls=%async_computation | async-start | bytes 524288 | tf_op jit(solution)/shard_map/all_to_all | solution.py:99
  101.8 10.0 %copy-start.3 = (f32[2048]{0:T(1024)S(1)}, f32[2048]{0:T(1024)}, u32[]{:S(2)}) copy-start(f32[2048]{0:T(1024)} %param.25) | copy-start | bytes 24580
  341.9 11.0 %copy-start.6 = (f32[128,2]{0,1:T(2,128)S(1)}, f32[128,2]{0,1:T(2,128)}, u32[]{:S(2)}) copy-start(f32[128,2]{0,1:T(2,128)} %param.28) | copy-start | bytes 3076
  347.1 35.7 %all-to-all-start.2 = ((bf16[128,3,2048]{2,1,0:T(4,128)(2,1)}), bf16[128,3,2048]{2,1,0:T(4,128)(2,1)}, u32[]{:S(2)}, u32[]{:S(2)}) async-start(bf16[128,3,2048]{2,1,0:T(4,128)(2,1)} %reshape.152), calls=%async_computation.2 | async-start | bytes 4194304 | tf_op jit(solution)/shard_map/all_to_all | solution.py:124
  392.8 8.4 %copy-start.4 = (f32[2048]{0:T(1024)S(1)}, f32[2048]{0:T(1024)}, u32[]{:S(2)}) copy-start(f32[2048]{0:T(1024)} %param.26) | copy-start | bytes 24580
Sparse Core Ops, SparseCore 0:
  9.9 73.9 all-gather.1
where the time goes:
time: 411 us; the launch traced here: 409 us
  blocking collectives  203 us (49%)
  waiting for transfers between devices  107 us (26%)
  local copies, waits for them, and re-layouts  45.1 us (11%)
  matrix products  17.9 us (4%)
  between operations  13.6 us (3%)
  other arithmetic  11.7 us (3%)
  starting transfers between devices  10.9 us (3%)
    all_to_all x1, blocking collectives, local(): lax.all_to_all(outgoing, ('sp', 'tp'), split_axis=0, concat_axis=0, tiled...  203 us
    all_gather x1, waiting for transfers between devices, local(): piece = lax.all_gather(paired, 'sp', axis=1, tiled=True)  70.6 us
    all_to_all x1, waiting for transfers between devices, local(): lax.all_to_all(expert_out.reshape(sources, slots, width_here), ('sp', 'tp...  29.7 us
  transfers between devices with their start and end apart: 3, of which 3 were waited for; matrix products, arithmetic and copies ran while one was open for 1% of the time, Pallas kernels for 0%

commit v1 on v0

--- a/solution.py
+++ b/solution.py
@@ -1,3 +1,4 @@
+import functools
 import math
 import jax
 import jax.numpy as jnp
@@ -7,6 +8,25 @@
 HEAD_DIM = 64
 NORM_EPS = 1e-06
 MASKED = -1e30
+
+
+def match_area_over_axis(packet, a_name):
+    pages = [packet]
+    n_shards = lax.axis_size(a_name)
+    for p in range(n_shards - 1):
+        pages.append(
+            lax.ppermute(
+                pages[-1],
+                axis_name=a_name,
+                perm=[(nth, (nth + 1) % n_shards) for nth in range(n_shards)],
+            )
+        )
+    return jnp.roll(
+        jnp.concatenate(pages[::-1], 1), (lax.axis_index(a_name) + 1) * packet.shape[1], axis=1
+    )
+
+
+mix_indices = functools.partial(match_area_over_axis, a_name="sp")
 
 
 def rms_scale(rows, gain):
@@ -77,7 +97,7 @@
         )
 
     running = initial
-    piece = lax.all_gather(paired, "sp", axis=1, tiled=True)
+    piece = mix_indices(paired)
     row_count = piece.shape[1]
     span_rows = math.gcd(row_count, tok_dev)
 

time: 411 us -> 609 us (1.48)
  waiting for transfers between devices: 107 us -> 242 us
  local copies, waits for them, and re-layouts: 45.1 us -> 105 us
  starting transfers between devices: 10.9 us -> 27.7 us
  between operations: 13.6 us -> 0.39 us
    ppermute x0 -> x15, waiting for transfers between devices: none -> 206 us  [match_area_over_axis(): lax.ppermute(pages[-1], axis_name=a_name, perm=[(nth, (nth + 1) % n_shard...]
    all_gather x1 -> x0, waiting for transfers between devices: 70.6 us -> none  [local(): piece = lax.all_gather(paired, 'sp', axis=1, tiled=True)]
    unnamed x21 -> x95, local copies, waits for them, and re-layouts: 4.41 us -> 56.6 us
    all_to_all x1, starting transfers between devices: 5.12 us -> 19.7 us  [local(): lax.all_to_all(attended, 'tp', split_axis=0, concat_axis=1, tiled=True)]
    dynamic_slice x0 -> x1, local copies, waits for them, and re-layouts: none -> 7.54 us  [match_area_over_axis(): jnp.roll(jnp.concatenate(pages[::-1], 1), (lax.axis_index(a_name) + 1) *...]
  transfers between devices with their start and end apart: 3 -> 17, of which waited for: 3 -> 17; matrix products, arithmetic and copies ran while one was open for 1% -> 1% of each run, Pallas kernels for 0% -> 0%
where the time goes in v1:
time: 609 us; the launch traced here: 606 us
  waiting for transfers between devices  242 us (40%)
  blocking collectives  199 us (33%)
  local copies, waits for them, and re-layouts  105 us (17%)
  starting transfers between devices  27.7 us (5%)
  matrix products  17.9 us (3%)
  other arithmetic  13.8 us (2%)
    ppermute x15, waiting for transfers between devices, match_area_over_axis(): lax.ppermute(pages[-1], axis_name=a_name, perm=[(nth, (nth + 1) % n_shard...  206 us
    all_to_all x1, blocking collectives, local(): lax.all_to_all(outgoing, ('sp', 'tp'), split_axis=0, concat_axis=0, tiled...  199 us
    unnamed x95, local copies, waits for them, and re-layouts  56.6 us
    all_to_all x1, waiting for transfers between devices, local(): lax.all_to_all(expert_out.reshape(sources, slots, width_here), ('sp', 'tp...  29.7 us
    all_to_all x1, starting transfers between devices, local(): lax.all_to_all(attended, 'tp', split_axis=0, concat_axis=1, tiled=True)  19.7 us
  transfers between devices with their start and end apart: 17, of which 17 were waited for; matrix products, arithmetic and copies ran while one was open for 1% of the time, Pallas kernels for 0%

profile of v1, /device:TPU:1, one launch (start us, length us, event | category | flops | bytes accessed | tf_op | source)
XLA Modules:
  0.0 606.2 jit_solution(13365848513844439057)
XLA Ops:
  4.5 16.4 %collective-permute-done = bf16[2,1024,128]{1,2,0:T(8,128)(2,1)S(1)} collective-permute-done((bf16[2,1024,128]{1,2,0:T(8,128)(2,1)S(1)}, bf16[2,1024,128]{1,2,0:T(8,128)(2,1)S(1)}, u32[]{:S(2)}, u32[]{:S(2)}) %collective-permute-start) | collective-permute-done | bytes 524320 | tf_op jit(solution)/shard_map/ppermute | solution.py:18
  20.9 15.5 %collective-permute-done.1 = bf16[2,1024,128]{1,2,0:T(8,128)(2,1)S(1)} collective-permute-done((bf16[2,1024,128]{1,2,0:T(8,128)(2,1)S(1)}, bf16[2,1024,128]{1,2,0:T(8,128)(2,1)S(1)}, u32[]{:S(2)}, u32[]{:S(2)}) %collective-permute-start.1) | collective-permute-done | bytes 524320 | tf_op jit(solution)/shard_map/ppermute | solution.py:18
  37.2 14.7 %collective-permute-done.2 = bf16[2,1024,128]{1,2,0:T(8,128)(2,1)S(1)} collective-permute-done((bf16[2,1024,128]{1,2,0:T(8,128)(2,1)S(1)}, bf16[2,1024,128]{1,2,0:T(8,128)(2,1)S(1)}, u32[]{:S(2)}, u32[]{:S(2)}) %collective-permute-start.2) | collective-permute-done | bytes 524320 | tf_op jit(solution)/shard_map/ppermute | solution.py:18
  52.7 13.8 %collective-permute-done.3 = bf16[2,1024,128]{1,2,0:T(8,128)(2,1)S(1)} collective-permute-done((bf16[2,1024,128]{1,2,0:T(8,128)(2,1)S(1)}, bf16[2,1024,128]{1,2,0:T(8,128)(2,1)S(1)}, u32[]{:S(2)}, u32[]{:S(2)}) %collective-permute-start.3) | collective-permute-done | bytes 524320 | tf_op jit(solution)/shard_map/ppermute | solution.py:18
  67.4 13.0 %collective-permute-done.4 = bf16[2,1024,128]{1,2,0:T(8,128)(2,1)S(1)} collective-permute-done((bf16[2,1024,128]{1,2,0:T(8,128)(2,1)S(1)}, bf16[2,1024,128]{1,2,0:T(8,128)(2,1)S(1)}, u32[]{:S(2)}, u32[]{:S(2)}) %collective-permute-start.4) | collective-permute-done | bytes 524320 | tf_op jit(solution)/shard_map/ppermute | solution.py:18
  81.2 12.1 %collective-permute-done.5 = bf16[2,1024,128]{1,2,0:T(8,128)(2,1)S(1)} collective-permute-done((bf16[2,1024,128]{1,2,0:T(8,128)(2,1)S(1)}, bf16[2,1024,128]{1,2,0:T(8,128)(2,1)S(1)}, u32[]{:S(2)}, u32[]{:S(2)}) %collective-permute-start.5) | collective-permute-done | bytes 524320 | tf_op jit(solution)/shard_map/ppermute | solution.py:18
  94.1 11.3 %collective-permute-done.6 = bf16[2,1024,128]{1,2,0:T(8,128)(2,1)S(1)} collective-permute-done((bf16[2,1024,128]{1,2,0:T(8,128)(2,1)S(1)}, bf16[2,1024,128]{1,2,0:T(8,128)(2,1)S(1)}, u32[]{:S(2)}, u32[]{:S(2)}) %collective-permute-start.6) | collective-permute-done | bytes 524320 | tf_op jit(solution)/shard_map/ppermute | solution.py:18
  106.3 11.3 %collective-permute-done.7 = bf16[2,1024,128]{1,2,0:T(8,128)(2,1)S(1)} collective-permute-done((bf16[2,1024,128]{1,2,0:T(8,128)(2,1)S(1)}, bf16[2,1024,128]{1,2,0:T(8,128)(2,1)S(1)}, u32[]{:S(2)}, u32[]{:S(2)}) %collective-permute-start.7) | collective-permute-done | bytes 524320 | tf_op jit(solution)/shard_map/ppermute | solution.py:18
  118.4 11.9 %collective-permute-done.8 = bf16[2,1024,128]{1,2,0:T(8,128)(2,1)S(1)} collective-permute-done((bf16[2,1024,128]{1,2,0:T(8,128)(2,1)S(1)}, bf16[2,1024,128]{1,2,0:T(8,128)(2,1)S(1)}, u32[]{:S(2)}, u32[]{:S(2)}) %collective-permute-start.8) | collective-permute-done | bytes 524320 | tf_op jit(solution)/shard_map/ppermute | solution.py:18
  131.2 13.1 %collective-permute-done.9 = bf16[2,1024,128]{1,2,0:T(8,128)(2,1)S(1)} collective-permute-done((bf16[2,1024,128]{1,2,0:T(8,128)(2,1)S(1)}, bf16[2,1024,128]{1,2,0:T(8,128)(2,1)S(1)}, u32[]{:S(2)}, u32[]{:S(2)}) %collective-permute-start.9) | collective-permute-done | bytes 524320 | tf_op jit(solution)/shard_map/ppermute | solution.py:18
  145.1 14.2 %collective-permute-done.10 = bf16[2,1024,128]{1,2,0:T(8,128)(2,1)S(1)} collective-permute-done((bf16[2,1024,128]{1,2,0:T(8,128)(2,1)S(1)}, bf16[2,1024,128]{1,2,0:T(8,128)(2,1)S(1)}, u32[]{:S(2)}, u32[]{:S(2)}) %collective-permute-start.10) | collective-permute-done | bytes 524320 | tf_op jit(solution)/shard_map/ppermute | solution.py:18
  160.1 15.4 %collective-permute-done.11 = bf16[2,1024,128]{1,2,0:T(8,128)(2,1)S(1)} collective-permute-done((bf16[2,1024,128]{1,2,0:T(8,128)(2,1)S(1)}, bf16[2,1024,128]{1,2,0:T(8,128)(2,1)S(1)}, u32[]{:S(2)}, u32[]{:S(2)}) %collective-permute-start.11) | collective-permute-done | bytes 524320 | tf_op jit(solution)/shard_map/ppermute | solution.py:18
  176.3 16.6 %collective-permute-done.12 = bf16[2,1024,128]{1,2,0:T(8,128)(2,1)} collective-permute-done((bf16[2,1024,128]{1,2,0:T(8,128)(2,1)S(1)}, bf16[2,1024,128]{1,2,0:T(8,128)(2,1)}, u32[]{:S(2)}, u32[]{:S(2)}) %collective-permute-start.12) | collective-permute-done | bytes 524320 | tf_op jit(solution)/shard_map/ppermute | solution.py:18
  194.3 15.1 %collective-permute-done.13 = bf16[2,1024,128]{1,2,0:T(8,128)(2,1)} collective-permute-done((bf16[2,1024,128]{1,2,0:T(8,128)(2,1)}, bf16[2,1024,128]{1,2,0:T(8,128)(2,1)}, u32[]{:S(2)}, u32[]{:S(2)}) %collective-permute-start.13) | collective-permute-done | bytes 524320 | tf_op jit(solution)/shard_map/ppermute | solution.py:18
  213.8 11.1 %collective-permute-done.14 = bf16[2,1024,128]{1,2,0:T(8,128)(2,1)} collective-permute-done((bf16[2,1024,128]{1,2,0:T(8,128)(2,1)}, bf16[2,1024,128]{1,2,0:T(8,128)(2,1)}, u32[]{:S(2)}, u32[]{:S(2)}) %collective-permute-start.14) | collective-permute-done | bytes 524320 | tf_op jit(solution)/shard_map/ppermute | solution.py:18
  269.2 7.5 %constant_dynamic-slice_fusion.4 = bf16[2,16384,128]{1,2,0:T(8,128)(2,1)} fusion(bf16[2,32768,128]{1,2,0:T(8,128)(2,1)} %constant_dynamic-update-slice_fusion, s32[]{:T(128)S(6)} %select_n.55), kind=kLoop, calls=%fused_computation.101 | loop fusion | bytes 16777220 | tf_op jit(solution)/shard_map/jit(_roll_dynamic)/dynamic_slice | solution.py:24
  276.8 11.8 %while.18 = (s32[]{:T(128)}, f32[2,1024]{1,0:T(2,128)S(1)}, f32[2,1024]{1,0:T(2,128)S(1)}, f32[1024,2,64]{0,2,1:T(8,128)S(1)}, s32[]{:T(128)}, /*index=5*/s32[]{...) while((s32[]{:T(128)}, f32[2,1024]{1,0:T(2,128)S(1)}, ...), condition=%wide.region_5.6_spmd, body=%wide.region_0.5_spmd.sunk | while | flops 578035712 | bytes 32457040 | solution.py:114
  276.9 11.2 %conditional.2 = ((f32[2,1024]{1,0:T(2,128)S(1)}, f32[2,1024]{1,0:T(2,128)S(1)}, f32[1024,2,64]{0,2,1:T(8,128)S(1)})) conditional(s32[]{:T(128)} %convert_element_type.89, (f32[2,1024]{1,0:T(2,128)S(1)}, f32[2,1024]{1,0:T(2,128)S(1)}, f32[1024,2,64]{0,2,1:T(8,128)S(1)}) %tuple.52, (s32[]{:T(128)}, s32[]{:T(128)}, bf16[2,16384,128]{1,2,0:T(8,128)(2,1)}, ...), branch_computations={%region_1.1_spmd, %region_2.4_spmd} | conditional | flops 578035712 | bytes 32456802 | solution.py:107
  289.5 19.7 %all-to-all-start = ((bf16[8,128,128]{1,2,0:T(8,128)(2,1)}), bf16[8,128,128]{1,2,0:T(8,128)(2,1)S(1)}, u32[]{:S(2)}, u32[]{:S(2)}) async-start(bf16[8,128,128]{1,2,0:T(8,128)(2,1)} %copy.45), calls=%async_computation | async-start | bytes 524288 | tf_op jit(solution)/shard_map/all_to_all | solution.py:119
  309.5 6.2 %all-to-all-done = bf16[8,128,128]{1,2,0:T(8,128)(2,1)S(1)} async-done(((bf16[8,128,128]{1,2,0:T(8,128)(2,1)}), bf16[8,128,128]{1,2,0:T(8,128)(2,1)S(1)}, u32[]{:S(2)}, u32[]{:S(2)}) %all-to-all-start) | async-done | bytes 262176 | tf_op jit(solution)/shard_map/all_to_all | solution.py:119
  332.5 199.1 %all_to_all.29 = bf16[128,3,2048]{2,1,0:T(4,128)(2,1)} all-to-all(bf16[128,3,2048]{2,1,0:T(4,128)(2,1)} %reshape.150), channel_id=1, replica_groups=mesh['sp'=16,'tp'=8] {'sp','tp'}, dimensions={0} | all-to-all | bytes 3145728 | tf_op jit(solution)/shard_map/all_to_all | solution.py:137
  540.7 5.3 convolution_convert_fusion
  551.1 5.8 all-to-all-start.2
  557.1 29.7 %all-to-all-done.2 = bf16[128,3,2048]{2,1,0:T(4,128)(2,1)} async-done(((bf16[128,3,2048]{2,1,0:T(4,128)(2,1)}), bf16[128,3,2048]{2,1,0:T(4,128)(2,1)}, u32[]{:S(2)}, u32[]{:S(2)}) %all-to-all-start.2) | async-done | bytes 1572896 | tf_op jit(solution)/shard_map/all_to_all | solution.py:144
  (180 shorter events, 126.0 us)
Async XLA Ops:
  0.0 540.6 %copy-start = (bf16[1,512,2048]{2,1,0:T(8,128)(2,1)S(1)}, bf16[1,512,2048]{2,1,0:T(8,128)(2,1)}, u32[]{:S(2)}) copy-start(bf16[1,512,2048]{2,1,0:T(8,128)(2,1)} %param.31) | copy-start | bytes 6291460
  2.4 18.5 %collective-permute-start = (bf16[2,1024,128]{1,2,0:T(8,128)(2,1)S(1)}, bf16[2,1024,128]{1,2,0:T(8,128)(2,1)S(1)}, u32[]{:S(2)}, u32[]{:S(2)}) collective-permute-start(bf16[2,1024,128]{1,2,0:T(8,128)(2,1)S(1)} %pad_maximum_fusion), channel_id=1, source_target_pairs={{0,8},{8,16},{16,24},{24,32},{32,40},{40,48},{48,56},{56,64},{64,7... | collective-permute-start | bytes 1572872 | tf_op jit(solution)/shard_map/ppermute | solution.py:18
  20.9 15.6 %collective-permute-start.1 = (bf16[2,1024,128]{1,2,0:T(8,128)(2,1)S(1)}, bf16[2,1024,128]{1,2,0:T(8,128)(2,1)S(1)}, u32[]{:S(2)}, u32[]{:S(2)}) collective-permute-start(bf16[2,1024,128]{1,2,0:T(8,128)(2,1)S(1)} %collective-permute-done), channel_id=1, source_target_pairs={{0,8},{8,16},{16,24},{24,32},{32,40},{40,48},{48,56},{56,64},{64,7... | collective-permute-start | bytes 1572872 | tf_op jit(solution)/shard_map/ppermute | solution.py:18
  37.2 14.7 %collective-permute-start.2 = (bf16[2,1024,128]{1,2,0:T(8,128)(2,1)S(1)}, bf16[2,1024,128]{1,2,0:T(8,128)(2,1)S(1)}, u32[]{:S(2)}, u32[]{:S(2)}) collective-permute-start(bf16[2,1024,128]{1,2,0:T(8,128)(2,1)S(1)} %collective-permute-done.1), channel_id=1, source_target_pairs={{0,8},{8,16},{16,24},{24,32},{32,40},{40,48},{48,56},{56,64},{64,7... | collective-permute-start | bytes 1572872 | tf_op jit(solution)/shard_map/ppermute | solution.py:18
  52.7 13.8 %collective-permute-start.3 = (bf16[2,1024,128]{1,2,0:T(8,128)(2,1)S(1)}, bf16[2,1024,128]{1,2,0:T(8,128)(2,1)S(1)}, u32[]{:S(2)}, u32[]{:S(2)}) collective-permute-start(bf16[2,1024,128]{1,2,0:T(8,128)(2,1)S(1)} %collective-permute-done.2), channel_id=1, source_target_pairs={{0,8},{8,16},{16,24},{24,32},{32,40},{40,48},{48,56},{56,64},{64,7... | collective-permute-start | bytes 1572872 | tf_op jit(solution)/shard_map/ppermute | solution.py:18
  67.4 13.0 %collective-permute-start.4 = (bf16[2,1024,128]{1,2,0:T(8,128)(2,1)S(1)}, bf16[2,1024,128]{1,2,0:T(8,128)(2,1)S(1)}, u32[]{:S(2)}, u32[]{:S(2)}) collective-permute-start(bf16[2,1024,128]{1,2,0:T(8,128)(2,1)S(1)} %collective-permute-done.3), channel_id=1, source_target_pairs={{0,8},{8,16},{16,24},{24,32},{32,40},{40,48},{48,56},{56,64},{64,7... | collective-permute-start | bytes 1572872 | tf_op jit(solution)/shard_map/ppermute | solution.py:18
  81.1 12.1 %collective-permute-start.5 = (bf16[2,1024,128]{1,2,0:T(8,128)(2,1)S(1)}, bf16[2,1024,128]{1,2,0:T(8,128)(2,1)S(1)}, u32[]{:S(2)}, u32[]{:S(2)}) collective-permute-start(bf16[2,1024,128]{1,2,0:T(8,128)(2,1)S(1)} %collective-permute-done.4), channel_id=1, source_target_pairs={{0,8},{8,16},{16,24},{24,32},{32,40},{40,48},{48,56},{56,64},{64,7... | collective-permute-start | bytes 1572872 | tf_op jit(solution)/shard_map/ppermute | solution.py:18
  94.1 11.4 %collective-permute-start.6 = (bf16[2,1024,128]{1,2,0:T(8,128)(2,1)S(1)}, bf16[2,1024,128]{1,2,0:T(8,128)(2,1)S(1)}, u32[]{:S(2)}, u32[]{:S(2)}) collective-permute-start(bf16[2,1024,128]{1,2,0:T(8,128)(2,1)S(1)} %collective-permute-done.5), channel_id=1, source_target_pairs={{0,8},{8,16},{16,24},{24,32},{32,40},{40,48},{48,56},{56,64},{64,7... | collective-permute-start | bytes 1572872 | tf_op jit(solution)/shard_map/ppermute | solution.py:18
  106.3 11.4 %collective-permute-start.7 = (bf16[2,1024,128]{1,2,0:T(8,128)(2,1)S(1)}, bf16[2,1024,128]{1,2,0:T(8,128)(2,1)S(1)}, u32[]{:S(2)}, u32[]{:S(2)}) collective-permute-start(bf16[2,1024,128]{1,2,0:T(8,128)(2,1)S(1)} %collective-permute-done.6), channel_id=1, source_target_pairs={{0,8},{8,16},{16,24},{24,32},{32,40},{40,48},{48,56},{56,64},{64,7... | collective-permute-start | bytes 1572872 | tf_op jit(solution)/shard_map/ppermute | solution.py:18
  118.4 11.9 %collective-permute-start.8 = (bf16[2,1024,128]{1,2,0:T(8,128)(2,1)S(1)}, bf16[2,1024,128]{1,2,0:T(8,128)(2,1)S(1)}, u32[]{:S(2)}, u32[]{:S(2)}) collective-permute-start(bf16[2,1024,128]{1,2,0:T(8,128)(2,1)S(1)} %collective-permute-done.7), channel_id=1, source_target_pairs={{0,8},{8,16},{16,24},{24,32},{32,40},{40,48},{48,56},{56,64},{64,7... | collective-permute-start | bytes 1572872 | tf_op jit(solution)/shard_map/ppermute | solution.py:18
  131.2 13.1 %collective-permute-start.9 = (bf16[2,1024,128]{1,2,0:T(8,128)(2,1)S(1)}, bf16[2,1024,128]{1,2,0:T(8,128)(2,1)S(1)}, u32[]{:S(2)}, u32[]{:S(2)}) collective-permute-start(bf16[2,1024,128]{1,2,0:T(8,128)(2,1)S(1)} %collective-permute-done.8), channel_id=1, source_target_pairs={{0,8},{8,16},{16,24},{24,32},{32,40},{40,48},{48,56},{56,64},{64,7... | collective-permute-start | bytes 1572872 | tf_op jit(solution)/shard_map/ppermute | solution.py:18
  145.1 14.2 %collective-permute-start.10 = (bf16[2,1024,128]{1,2,0:T(8,128)(2,1)S(1)}, bf16[2,1024,128]{1,2,0:T(8,128)(2,1)S(1)}, u32[]{:S(2)}, u32[]{:S(2)}) collective-permute-start(bf16[2,1024,128]{1,2,0:T(8,128)(2,1)S(1)} %collective-permute-done.9), channel_id=1, source_target_pairs={{0,8},{8,16},{16,24},{24,32},{32,40},{40,48},{48,56},{56,64},{64,7... | collective-permute-start | bytes 1572872 | tf_op jit(solution)/shard_map/ppermute | solution.py:18
  160.1 15.4 %collective-permute-start.11 = (bf16[2,1024,128]{1,2,0:T(8,128)(2,1)S(1)}, bf16[2,1024,128]{1,2,0:T(8,128)(2,1)S(1)}, u32[]{:S(2)}, u32[]{:S(2)}) collective-permute-start(bf16[2,1024,128]{1,2,0:T(8,128)(2,1)S(1)} %collective-permute-done.10), channel_id=1, source_target_pairs={{0,8},{8,16},{16,24},{24,32},{32,40},{40,48},{48,56},{56,64},{64,7... | collective-permute-start | bytes 1572872 | tf_op jit(solution)/shard_map/ppermute | solution.py:18
  176.3 16.6 %collective-permute-start.12 = (bf16[2,1024,128]{1,2,0:T(8,128)(2,1)S(1)}, bf16[2,1024,128]{1,2,0:T(8,128)(2,1)}, u32[]{:S(2)}, u32[]{:S(2)}) collective-permute-start(bf16[2,1024,128]{1,2,0:T(8,128)(2,1)S(1)} %collective-permute-done.11), channel_id=1, source_target_pairs={{0,8},{8,16},{16,24},{24,32},{32,40},{40,48},{48,56},{56,64},{64,7... | collective-permute-start | bytes 1572872 | tf_op jit(solution)/shard_map/ppermute | solution.py:18
  193.0 16.4 %collective-permute-start.13 = (bf16[2,1024,128]{1,2,0:T(8,128)(2,1)}, bf16[2,1024,128]{1,2,0:T(8,128)(2,1)}, u32[]{:S(2)}, u32[]{:S(2)}) collective-permute-start(bf16[2,1024,128]{1,2,0:T(8,128)(2,1)} %collective-permute-done.12), channel_id=1, source_target_pairs={{0,8},{8,16},{16,24},{24,32},{32,40},{40,48},{48,56},{56,64},{64,7... | collective-permute-start | bytes 1572872 | tf_op jit(solution)/shard_map/ppermute | solution.py:18
  209.3 15.5 %collective-permute-start.14 = (bf16[2,1024,128]{1,2,0:T(8,128)(2,1)}, bf16[2,1024,128]{1,2,0:T(8,128)(2,1)}, u32[]{:S(2)}, u32[]{:S(2)}) collective-permute-start(bf16[2,1024,128]{1,2,0:T(8,128)(2,1)} %collective-permute-done.13), channel_id=1, source_target_pairs={{0,8},{8,16},{16,24},{24,32},{32,40},{40,48},{48,56},{56,64},{64,7... | collective-permute-start | bytes 1572872 | tf_op jit(solution)/shard_map/ppermute | solution.py:18
  211.4 52.8 %copy-start.8 = (bf16[2,1024,128]{1,2,0:T(8,128)(2,1)S(1)}, bf16[2,1024,128]{1,2,0:T(8,128)(2,1)}, u32[]{:S(2)}) copy-start(bf16[2,1024,128]{1,2,0:T(8,128)(2,1)} %copy-done.7) | copy-start | bytes 1572868
  211.5 53.6 %copy-start.6 = (bf16[2,1024,128]{1,2,0:T(8,128)(2,1)S(1)}, bf16[2,1024,128]{1,2,0:T(8,128)(2,1)}, u32[]{:S(2)}) copy-start(bf16[2,1024,128]{1,2,0:T(8,128)(2,1)} %copy-done.5) | copy-start | bytes 1572868
  211.5 54.4 %copy-start.4 = (bf16[2,1024,128]{1,2,0:T(8,128)(2,1)S(1)}, bf16[2,1024,128]{1,2,0:T(8,128)(2,1)}, u32[]{:S(2)}) copy-start(bf16[2,1024,128]{1,2,0:T(8,128)(2,1)} %copy-done.3) | copy-start | bytes 1572868
  211.5 55.2 %copy-start.2 = (bf16[2,1024,128]{1,2,0:T(8,128)(2,1)S(1)}, bf16[2,1024,128]{1,2,0:T(8,128)(2,1)}, u32[]{:S(2)}) copy-start(bf16[2,1024,128]{1,2,0:T(8,128)(2,1)} %copy-done.1) | copy-start | bytes 1572868
  289.5 26.2 %all-to-all-start = ((bf16[8,128,128]{1,2,0:T(8,128)(2,1)}), bf16[8,128,128]{1,2,0:T(8,128)(2,1)S(1)}, u32[]{:S(2)}, u32[]{:S(2)}) async-start(bf16[8,128,128]{1,2,0:T(8,128)(2,1)} %copy.45), calls=%async_computation | async-start | bytes 524288 | tf_op jit(solution)/shard_map/all_to_all | solution.py:119
  332.5 224.4 %copy-start.28 = (f32[128,2]{0,1:T(2,128)S(1)}, f32[128,2]{0,1:T(2,128)}, u32[]{:S(2)}) copy-start(f32[128,2]{0,1:T(2,128)} %param.28) | copy-start | bytes 3076
  546.0 59.2 %copy-start.27 = (f32[2048]{0:T(1024)S(1)}, f32[2048]{0:T(1024)}, u32[]{:S(2)}) copy-start(f32[2048]{0:T(1024)} %param.26) | copy-start | bytes 24580
  551.1 35.7 %all-to-all-start.2 = ((bf16[128,3,2048]{2,1,0:T(4,128)(2,1)}), bf16[128,3,2048]{2,1,0:T(4,128)(2,1)}, u32[]{:S(2)}, u32[]{:S(2)}) async-start(bf16[128,3,2048]{2,1,0:T(4,128)(2,1)} %reshape.152), calls=%async_computation.2 | async-start | bytes 4194304 | tf_op jit(solution)/shard_map/all_to_all | solution.py:144
  (22 other events, 503.6 us)
